TPU v7x, 256 devices: a 4x2x16 block of a 4x16x16 slice. The times are simulated.
256 devices in a mesh: grp: 2 (over y), ep: 32 (over z, core), tp: 4 (over x).
Axes of the slice: x: 4, y: 2, z: 16, core: 2. Of those that a mesh axis runs over, the one named last changes fastest.
The devices are a block of a 4x16x16 slice.
Arguments:
- outer_gate: bfloat16 [32768, 1024], P(('grp', 'ep'), 'tp'), parts along dimension 0, may hold values from -6 to 6
- inner_gate: bfloat16 [32768, 1024], P(('grp', 'ep'), 'tp'), parts along dimension 0, may hold values from -6 to 6
- conv_input: bfloat16 [32768, 1024], P(('grp', 'ep'), 'tp'), parts along dimension 0, may hold values from -6 to 6
- conv_taps: float32 [3, 1024], P(None, 'tp'), may hold values from -3.5 to 3.5
- mixer_weight: bfloat16 [1024, 2048], P('tp'), may hold values from -0.1875 to 0.1875
- expert_input: bfloat16 [32768, 2048], P(('grp', 'ep', 'tp')), parts along dimension 0, may hold values from -6 to 6
- norm_gain: float32 [2048], replicated, may hold values from 0.1 to 1.9
- expert_ids: int32 [32768, 2], P(('grp', 'ep', 'tp')), parts along dimension 0, may hold values from 0 to 31, all different within a row; in each aligned block of 128 rows (0 to 127, 128 to 255, ...) at most 10 rows name the same one
- route_weight: float32 [32768, 2], P(('grp', 'ep', 'tp')), parts along dimension 0, may hold values from 0.25 to 1
- gate_weight: bfloat16 [32, 2048, 3072], P('ep', None, 'tp'), may hold values from -0.125 to 0.125
- up_weight: bfloat16 [32, 2048, 3072], P('ep', None, 'tp'), may hold values from -0.125 to 0.125
- down_weight: bfloat16 [32, 3072, 2048], P('ep', 'tp'), may hold values from -0.109375 to 0.109375
Outputs:
- mixer_output: bfloat16 [32768, 2048], P(('grp', 'ep', 'tp')), parts along dimension 0
- expert_output: bfloat16 [32768, 2048], P(('grp', 'ep', 'tp')), parts along dimension 0
There are 2 independent parts, one for each index of `grp`. A program takes and returns all parts, laid end to end along the dimension named above; an argument that names none is the same for every part. Nothing has to cross between parts.
Inputs may be any that keep to these rules, and one draw needn't show every extreme that they name: `expert_ids`: each row names 2 different experts. Among the rows of one device no expert is named more than 10 times, a bound that some block reaches.
All inputs are finite; a program needn't handle non-finite values.
Results may differ from a plain program's by a relative error of at most 0.011.
Values may be sent and summed in bfloat16 or wider, within the bound.
A program may use at most 128 MiB of HBM per device.

v0:
```python
import jax
import jax.numpy as jnp
from jax import lax
from jax.sharding import Mesh
from jax.sharding import PartitionSpec as P

TAPS = 3
EP = ("ep_0", "ep_1")
GRP_EP = ("grp", "ep_0", "ep_1")
GRP_EP_TP = ("grp", "ep_0", "ep_1", "tp")
epsilon = 1e-06


def shifted(value, axis, steps):
    count = lax.axis_size(axis)
    initial, last = (max(0, -steps), min(count, count - steps))
    return lax.ppermute(value, axis, [(source, source + steps) for source in range(initial, last)])


def split_up(value, dim, peers):
    lengths = value.shape
    tiles = value.reshape(*lengths[:dim], peers, lengths[dim] // peers, *lengths[dim + 1 :])
    return jnp.moveaxis(tiles, dim, 0)


def summed_on_arrival(value, axis, dim):
    tiles = split_up(value, dim, lax.axis_size(axis))
    arrived = lax.all_to_all(tiles, axis, split_axis=0, concat_axis=0, tiled=True)
    return arrived.astype(jnp.float32).sum(axis=0)


def laid_out(tiles, dim):
    tiles = jnp.moveaxis(tiles, 0, dim)
    lengths = tiles.shape
    return tiles.reshape(*lengths[:dim], lengths[dim] * lengths[dim + 1], *lengths[dim + 2 :])


def exchange_in_order(tiles, axes, order):
    lengths = [lax.axis_size(a) for a in axes]
    tiles = tiles.reshape(*lengths, *tiles.shape[1:])
    for k in order:
        tiles = lax.all_to_all(tiles, axes[k], split_axis=k, concat_axis=k, tiled=True)
    return tiles.reshape(-1, *tiles.shape[len(axes) :])


def two_step_exchange(value, groups, order, split_dim, concat_dim):
    peers = lax.axis_size(groups[0]) * lax.axis_size(groups[1])
    tiles = split_up(value, split_dim, peers)
    return laid_out(exchange_in_order(tiles, groups, order), concat_dim)


def on_device(
    outer_gate,
    inner_gate,
    conv_input,
    conv_taps,
    mixer_weight,
    expert_input,
    norm_gain,
    expert_ids,
    route_weight,
    gate_weight,
    up_weight,
    down_weight,
):
    gated_rows = inner_gate.astype(jnp.float32) * conv_input.astype(jnp.float32)
    length = gated_rows.shape[0]
    earlier = shifted(gated_rows[length - (TAPS - 1) :], EP, 1)
    padded = jnp.concatenate([earlier, gated_rows], axis=0)
    convolved = jnp.zeros_like(gated_rows)
    for tap_index in range(TAPS):
        convolved = convolved + conv_taps[tap_index] * padded[tap_index : tap_index + length]
    mixed = (outer_gate.astype(jnp.float32) * convolved).astype(jnp.bfloat16)
    mixer_output = summed_on_arrival(
        jnp.dot(mixed, mixer_weight, preferred_element_type=jnp.float32).astype(jnp.bfloat16),
        "tp",
        0,
    ).astype(jnp.bfloat16)
    inputs = expert_input.astype(jnp.float32)
    normed = (
        inputs * lax.rsqrt(jnp.mean(inputs * inputs, axis=1, keepdims=True) + epsilon) * norm_gain
    ).astype(jnp.bfloat16)
    tokens_here, top_count = expert_ids.shape
    model_width = expert_input.shape[1]
    expert_count = lax.axis_size(EP) * gate_weight.shape[0]
    capacity = 5 * tokens_here * top_count // (4 * expert_count)
    flat_ids = expert_ids.reshape(-1)
    one_hot = (flat_ids[:, None] == jnp.arange(expert_count, dtype=jnp.int32)[None, :]).astype(
        jnp.int32
    )
    ranks = jnp.sum((jnp.cumsum(one_hot, axis=0) - 1) * one_hot, axis=1)
    target = flat_ids * capacity + ranks
    duplicates = jnp.broadcast_to(
        normed[:, None, :], (tokens_here, top_count, model_width)
    ).reshape(-1, model_width)
    outgoing = (
        jnp.zeros((expert_count * capacity, model_width), jnp.bfloat16).at[target].set(duplicates)
    )
    gate_local = gate_weight[0]
    up_local = up_weight[0]
    down_local = down_weight[0]
    arrived = two_step_exchange(
        outgoing.reshape(expert_count, capacity, model_width), ("ep_0", "ep_1"), (1, 0), 0, 0
    )
    sources = arrived.shape[0]
    slot_count = arrived.shape[1]
    stacked = arrived.reshape(sources * slot_count, model_width)
    block_rows = lax.all_gather(stacked, "tp", axis=0, tiled=True)
    gate_value = jnp.dot(block_rows, gate_local, preferred_element_type=jnp.float32)
    up_value = jnp.dot(block_rows, up_local, preferred_element_type=jnp.float32)
    hidden = (jax.nn.silu(gate_value) * up_value).astype(jnp.bfloat16)
    own_sums = summed_on_arrival(
        jnp.dot(hidden, down_local, preferred_element_type=jnp.float32).astype(jnp.bfloat16),
        "tp",
        0,
    ).astype(jnp.bfloat16)
    answers = two_step_exchange(
        own_sums.reshape(sources, slot_count, model_width), ("ep_0", "ep_1"), (1, 0), 0, 0
    )
    picked = answers.reshape(expert_count * capacity, model_width)[target]
    picked = picked.astype(jnp.float32).reshape(tokens_here, top_count, model_width)
    expert_output = jnp.sum(picked * route_weight[:, :, None], axis=1).astype(jnp.bfloat16)
    return (mixer_output, expert_output)


def solution(mesh):
    finer = Mesh(
        mesh.devices.reshape(mesh.shape["grp"], 16, 2, mesh.shape["tp"]),
        ("grp", "ep_0", "ep_1", "tp"),
    )
    placed = (
        P(GRP_EP, "tp"),
        P(GRP_EP, "tp"),
        P(GRP_EP, "tp"),
        P(None, "tp"),
        P("tp", None),
        P(GRP_EP_TP, None),
        P(),
        P(GRP_EP_TP, None),
        P(GRP_EP_TP, None),
        P(EP, None, "tp"),
        P(EP, None, "tp"),
        P(EP, "tp", None),
    )
    return jax.shard_map(
        on_device,
        mesh=finer,
        in_specs=placed,
        out_specs=(P(GRP_EP_TP, None), P(GRP_EP_TP, None)),
        check_vma=False,
    )
```

profile of v0, /device:TPU:40, one launch (start us, length us, event | category | flops | bytes accessed | tf_op | source)
XLA Modules:
  0.0 410.6 jit_solution(17758050569771702696)
XLA Ops:
  7.2 0.0 copy-start
  7.2 0.1 all-gather.2.cloned.1.call-start
  7.3 0.9 copy.21
  8.2 0.1 eq.29
  8.3 0.1 eq.25
  8.5 0.7 broadcast_multiply_fusion
  9.2 0.6 reduce-window.6
  9.8 0.2 slice_reduce_fusion
  10.0 0.1 copy.20
  10.1 0.1 mul.102
  10.3 1.2 fusion.5
  11.5 1.2 fusion.7
  12.7 1.7 broadcast_in_dim.5
  14.4 2.3 reshape.93
  16.7 0.1 fusion.22
  16.8 4.0 scatter_custom_fusion
  20.7 3.3 reshape_reshape_reshape.12
  24.1 2.3 copy.24
  26.4 4.8 %all_to_all.30 = bf16[16,2,1,10,2048]{4,0,3,2,1:T(8,128)(2,1)S(1)} all-to-all(bf16[16,2,1,10,2048]{4,0,3,2,1:T(8,128)(2,1)S(1)} %copy.24), channel_id=1, replica_groups=mesh['grp'=2,'ep_0'=16,'ep_1'=2,'tp'=4] {'ep_1'}, dimensions={1} | all-to-all | bytes 2621440 | tf_op jit(solution)/shard_map/all_to_all | solution.py:42
  31.2 1.3 copy.25
  32.5 87.6 %all_to_all.31 = bf16[16,2,1,10,2048]{4,1,3,2,0:T(2,128)(2,1)S(1)} all-to-all(bf16[16,2,1,10,2048]{4,1,3,2,0:T(2,128)(2,1)S(1)} %copy.25), channel_id=1, replica_groups=mesh['grp'=2,'ep_0'=16,'ep_1'=2,'tp'=4] {'ep_0'}, dimensions={0} | all-to-all | bytes 2621440 | tf_op jit(solution)/shard_map/all_to_all | solution.py:42
  120.1 2.0 copy.26
  122.1 3.6 reshape_reshape_reshape.13
  125.7 0.1 all-gather.2.cloned.1.call-update
  125.8 58.0 %all-gather.2.cloned.1.call-done = bf16[1280,2048]{1,0:T(8,128)(2,1)} async-done(((bf16[320,2048]{1,0:T(8,128)(2,1)}), bf16[1280,2048]{1,0:T(8,128)(2,1)}) %all-gather.2.cloned.1.call-update) | async-done | bytes 5242896 | tf_op jit(solution)/shard_map/all_gather | solution.py:108
  183.7 0.0 copy-start.8
  183.7 0.0 copy-start.9
  183.7 7.2 %fusion.3 = f32[1280,768]{1,0:T(8,128)S(1)} fusion(bf16[1280,2048]{1,0:T(8,128)(2,1)} %all-gather.2.cloned.1.call-done, bf16[1,2048,768]{2,1,0:T(8,128)(2,1)} %param.21), kind=kOutput, calls=%fused_computation.7 | convolution fusion | flops 4026531840 | bytes 12320768 | tf_op jit(solution)/shard_map/dot_general | solution.py:109
  191.0 0.0 copy-done.8
  191.0 0.0 copy-done.9
  191.0 4.8 %fusion = bf16[1280,768]{1,0:T(8,128)(2,1)S(1)} fusion(bf16[1280,2048]{1,0:T(8,128)(2,1)S(1)} %copy-done.8, f32[1280,768]{1,0:T(8,128)S(1)} %fusion.3, bf16[1,2048,768]{2,1,0:T(8,128)(2,1)S(1)} %copy-done.9), kind=kOutput, calls=%fused_computation.4 | convolution fusion | flops 4032430080 | bytes 14286848 | tf_op jit(solution)/shard_map/dot_general | solution.py:110
  195.8 0.0 copy-done
  195.8 6.1 %convolution_convert_fusion = bf16[1280,2048]{1,0:T(8,128)(2,1)} fusion(bf16[1280,768]{1,0:T(8,128)(2,1)S(1)} %fusion, bf16[1,768,2048]{2,1,0:T(8,128)(2,1)S(1)} %copy-done), kind=kOutput, calls=%fused_computation.2 | convolution fusion | flops 4029153280 | bytes 10354688 | tf_op jit(solution)/shard_map/dot_general | solution.py:113
  201.9 0.0 copy-start.3
  201.9 5.3 %all-to-all-start.3 = ((bf16[4,320,2048]{2,1,0:T(8,128)(2,1)}), bf16[4,320,2048]{2,1,0:T(8,128)(2,1)}, u32[]{:S(2)}, u32[]{:S(2)}) async-start(bf16[4,320,2048]{2,1,0:T(8,128)(2,1)} %bitcast.39), calls=%async_computation.3 | async-start | bytes 10485760 | tf_op jit(solution)/shard_map/all_to_all | solution.py:28
  207.2 0.0 copy-done.4
  207.2 0.0 copy-done.5
  207.2 0.1 convert_multiply_fusion.2
  207.3 1.6 collective-permute-start
  208.9 0.0 copy-done.6
  208.9 0.8 collective-permute-done
  209.7 0.0 copy-done.2
  209.7 0.0 copy-done.3
  209.7 2.1 convolution_convert_fusion.1
  211.8 55.5 %all-to-all-done.3 = bf16[4,320,2048]{2,1,0:T(8,128)(2,1)} async-done(((bf16[4,320,2048]{2,1,0:T(8,128)(2,1)}), bf16[4,320,2048]{2,1,0:T(8,128)(2,1)}, u32[]{:S(2)}, u32[]{:S(2)}) %all-to-all-start.3) | async-done | bytes 5242912 | tf_op jit(solution)/shard_map/all_to_all | solution.py:28
  267.3 5.0 %reduce_sum.57 = bf16[320,2048]{1,0:T(8,128)(2,1)} reduce(bf16[4,320,2048]{2,1,0:T(8,128)(2,1)} %all-to-all-done.3, bf16[]{:T(256)} %constant.9.clone.1), dimensions={0}, to_apply=%region_6.7 | reduce | flops 1966080 | bytes 6553602 | tf_op jit(solution)/shard_map/reduce_sum | solution.py:29
  272.3 2.3 reshape_reshape_reshape.14
  274.6 0.7 copy.27
  275.4 5.6 %all_to_all.32 = bf16[16,2,1,10,2048]{4,0,3,2,1:T(8,128)(2,1)} all-to-all(bf16[16,2,1,10,2048]{4,0,3,2,1:T(8,128)(2,1)S(1)} %copy.27), channel_id=1, replica_groups=mesh['grp'=2,'ep_0'=16,'ep_1'=2,'tp'=4] {'ep_1'}, dimensions={1} | all-to-all | bytes 2621440 | tf_op jit(solution)/shard_map/all_to_all | solution.py:42
  281.0 3.9 all-to-all-start
  284.9 0.0 copy-start.7
  284.9 3.7 copy.28
  288.7 23.1 %all-to-all-done = bf16[4,128,2048]{2,1,0:T(8,128)(2,1)S(1)} async-done(((bf16[4,128,2048]{2,1,0:T(8,128)(2,1)}), bf16[4,128,2048]{2,1,0:T(8,128)(2,1)S(1)}, u32[]{:S(2)}, u32[]{:S(2)}) %all-to-all-start) | async-done | bytes 2097184 | tf_op jit(solution)/shard_map/all_to_all | solution.py:28
  311.8 12.4 %all-to-all-start.5 = ((bf16[16,2,1,10,2048]{4,1,3,2,0:T(2,128)(2,1)}), bf16[16,2,1,10,2048]{4,1,3,2,0:T(2,128)(2,1)}, u32[]{:S(2)}, u32[]{:S(2)}) async-start(bf16[16,2,1,10,2048]{4,1,3,2,0:T(2,128)(2,1)} %copy.28), calls=%async_computation.5 | async-start | bytes 2621440 | tf_op jit(solution)/shard_map/all_to_all | solution.py:42
  324.1 0.0 copy-done.7
  324.1 0.1 copy.30
  324.3 1.3 reduce_sum.53
  325.6 60.9 %all-to-all-done.5 = bf16[16,2,1,10,2048]{4,1,3,2,0:T(2,128)(2,1)} async-done(((bf16[16,2,1,10,2048]{4,1,3,2,0:T(2,128)(2,1)}), bf16[16,2,1,10,2048]{4,1,3,2,0:T(2,128)(2,1)}, u32[]{:S(2)}, u32[]{:S(2)}) %all-to-all-start.5) | async-done | bytes 1310752 | tf_op jit(solution)/shard_map/all_to_all | solution.py:42
  386.5 2.0 copy.29
  388.5 1.3 reshape_reshape_reshape.15
  389.8 5.0 %gather_fusion = bf16[256,2048]{1,0:T(8,128)(2,1)} fusion(bf16[320,2048]{1,0:T(8,128)(2,1)} %reshape_reshape_reshape.15, s32[1024]{0:T(1024)S(1)} %pad_clamp_fusion), kind=kCustom, calls=%fused_computation | custom fusion | bytes 2098176 | tf_op jit(solution)/shard_map/gather | solution.py:120
  394.8 3.4 reshape.80
  398.2 5.6 %multiply_reduce_fusion = bf16[128,2048]{1,0:T(8,128)(2,1)} fusion(f32[128,2,2048]{2,1,0:T(2,128)} %reshape.80, f32[128,2]{1,0:T(8,128)S(1)} %copy.30), kind=kLoop, calls=%fused_computation.10 | loop fusion | flops 786432 | bytes 2622464 | tf_op jit(solution)/shard_map/reduce_sum | solution.py:122
  403.8 0.0 copy-done.1
  (13 shorter events, 0.1 us)
Async XLA Ops:
  7.2 188.7 %copy-start = (bf16[1,768,2048]{2,1,0:T(8,128)(2,1)S(1)}, bf16[1,768,2048]{2,1,0:T(8,128)(2,1)}, u32[]{:S(2)}) copy-start(bf16[1,768,2048]{2,1,0:T(8,128)(2,1)} %param.23) | copy-start | bytes 9437188
  7.2 176.5 %all-gather.2.cloned.1.call-start = ((), (), s32[]{:S(2)}) async-start(), calls=%async_computation.6 | async-start | bytes 6553600 | tf_op jit(solution)/shard_map/all_gather | solution.py:108
  183.7 7.3 %copy-start.8 = (bf16[1280,2048]{1,0:T(8,128)(2,1)S(1)}, bf16[1280,2048]{1,0:T(8,128)(2,1)}, u32[]{:S(2)}) copy-start(bf16[1280,2048]{1,0:T(8,128)(2,1)} %all-gather.2.cloned.1.call-done) | copy-start | bytes 15728644
  183.7 7.3 %copy-start.9 = (bf16[1,2048,768]{2,1,0:T(8,128)(2,1)S(1)}, bf16[1,2048,768]{2,1,0:T(8,128)(2,1)}, u32[]{:S(2)}) copy-start(bf16[1,2048,768]{2,1,0:T(8,128)(2,1)} %param.22) | copy-start | bytes 9437188
  201.9 5.3 %copy-start.4 = (bf16[512,256]{1,0:T(8,128)(2,1)S(1)}, bf16[512,256]{1,0:T(8,128)(2,1)}, u32[]{:S(2)}) copy-start(bf16[512,256]{1,0:T(8,128)(2,1)} %param.14) | copy-start | bytes 786436
  201.9 5.3 %copy-start.5 = (bf16[512,256]{1,0:T(8,128)(2,1)S(1)}, bf16[512,256]{1,0:T(8,128)(2,1)}, u32[]{:S(2)}) copy-start(bf16[512,256]{1,0:T(8,128)(2,1)} %param.13) | copy-start | bytes 786436
  201.9 7.0 %copy-start.6 = (f32[3,256]{1,0:T(4,128)S(1)}, f32[3,256]{1,0:T(4,128)}, u32[]{:S(2)}) copy-start(f32[3,256]{1,0:T(4,128)} %param.15) | copy-start | bytes 9220
  201.9 7.8 %copy-start.2 = (bf16[256,2048]{1,0:T(8,128)(2,1)S(1)}, bf16[256,2048]{1,0:T(8,128)(2,1)}, u32[]{:S(2)}) copy-start(bf16[256,2048]{1,0:T(8,128)(2,1)} %param.16) | copy-start | bytes 3145732
  201.9 7.8 %copy-start.3 = (bf16[512,256]{1,0:T(8,128)(2,1)S(1)}, bf16[512,256]{1,0:T(8,128)(2,1)}, u32[]{:S(2)}) copy-start(bf16[512,256]{1,0:T(8,128)(2,1)} %param.12) | copy-start | bytes 786436
  201.9 65.4 %all-to-all-start.3 = ((bf16[4,320,2048]{2,1,0:T(8,128)(2,1)}), bf16[4,320,2048]{2,1,0:T(8,128)(2,1)}, u32[]{:S(2)}, u32[]{:S(2)}) async-start(bf16[4,320,2048]{2,1,0:T(8,128)(2,1)} %bitcast.39), calls=%async_computation.3 | async-start | bytes 10485760 | tf_op jit(solution)/shard_map/all_to_all | solution.py:28
  207.3 2.4 collective-permute-start
  281.0 30.7 %all-to-all-start = ((bf16[4,128,2048]{2,1,0:T(8,128)(2,1)}), bf16[4,128,2048]{2,1,0:T(8,128)(2,1)S(1)}, u32[]{:S(2)}, u32[]{:S(2)}) async-start(bf16[4,128,2048]{2,1,0:T(8,128)(2,1)} %bitcast.3), calls=%async_computation | async-start | bytes 4194304 | tf_op jit(solution)/shard_map/all_to_all | solution.py:28
  284.9 39.2 %copy-start.7 = (f32[128,2]{0,1:T(2,128)S(1)}, f32[128,2]{0,1:T(2,128)}, u32[]{:S(2)}) copy-start(f32[128,2]{0,1:T(2,128)} %param.20) | copy-start | bytes 3076
  311.8 74.7 %all-to-all-start.5 = ((bf16[16,2,1,10,2048]{4,1,3,2,0:T(2,128)(2,1)}), bf16[16,2,1,10,2048]{4,1,3,2,0:T(2,128)(2,1)}, u32[]{:S(2)}, u32[]{:S(2)}) async-start(bf16[16,2,1,10,2048]{4,1,3,2,0:T(2,128)(2,1)} %copy.28), calls=%async_computation.5 | async-start | bytes 2621440 | tf_op jit(solution)/shard_map/all_to_all | solution.py:42
  389.8 14.0 %copy-start.1 = (bf16[1,768,2048]{2,1,0:T(8,128)(2,1)S(1)}, bf16[1,768,2048]{2,1,0:T(8,128)(2,1)}, u32[]{:S(2)}) copy-start(bf16[1,768,2048]{2,1,0:T(8,128)(2,1)} %param.23) | copy-start | bytes 9437188
Sparse Core Ops, SparseCore 0:
  125.9 57.8 all-gather.1
where the time goes:
time: 412 us; the launch traced here: 411 us
  waiting for transfers between devices  198 us (48%)
  blocking collectives  98 us (24%)
  local copies, waits for them, and re-layouts  40.7 us (10%)
  starting transfers between devices  23.2 us (6%)
  matrix products  20.2 us (5%)
  other arithmetic  15.8 us (4%)
  between operations  14.3 us (3%)
    all_to_all x3, blocking collectives, exchange_in_order(): lax.all_to_all(tiles, axes[k], split_axis=k, concat_axis=k, tiled=True)  98 us
    all_to_all x2, waiting for transfers between devices, summed_on_arrival(): lax.all_to_all(tiles, axis, split_axis=0, concat_axis=0, tiled=True)  78.6 us
    all_to_all x1, waiting for transfers between devices, exchange_in_order(): lax.all_to_all(tiles, axes[k], split_axis=k, concat_axis=k, tiled=True)  60.9 us
    all_gather x1, waiting for transfers between devices, on_device(): block_rows = lax.all_gather(stacked, 'tp', axis=0, tiled=True)  58 us
    all_to_all x1, starting transfers between devices, exchange_in_order(): lax.all_to_all(tiles, axes[k], split_axis=k, concat_axis=k, tiled=True)  12.4 us
    all_to_all x2, starting transfers between devices, summed_on_arrival(): lax.all_to_all(tiles, axis, split_axis=0, concat_axis=0, tiled=True)  9.19 us
    all_to_all x4, local copies, waits for them, and re-layouts, exchange_in_order(): lax.all_to_all(tiles, axes[k], split_axis=k, concat_axis=k, tiled=True)  9.04 us
    another operation x4, local copies, waits for them, and re-layouts, exchange_in_order(): tiles = tiles.reshape(*lengths, *tiles.shape[1:])  8.68 us
  transfers between devices with their start and end apart: 5, of which 5 were waited for; matrix products, arithmetic and copies ran while one was open for 2% of the time, Pallas kernels for 0%

commit v1 on v0

--- a/solution.py
+++ b/solution.py
@@ -105,7 +105,8 @@
     sources = arrived.shape[0]
     slot_count = arrived.shape[1]
     stacked = arrived.reshape(sources * slot_count, model_width)
-    block_rows = lax.all_gather(stacked, "tp", axis=0, tiled=True)
+    copies = jnp.concatenate([stacked] * lax.axis_size("tp"), axis=0)
+    block_rows = lax.all_to_all(copies, "tp", 0, 0, tiled=True)
     gate_value = jnp.dot(block_rows, gate_local, preferred_element_type=jnp.float32)
     up_value = jnp.dot(block_rows, up_local, preferred_element_type=jnp.float32)
     hidden = (jax.nn.silu(gate_value) * up_value).astype(jnp.bfloat16)

time: 412 us -> 398 us (0.966)
  waiting for transfers between devices: 198 us -> 134 us
  blocking collectives: 98 us -> 157 us
  between operations: 14.3 us -> 0.86 us
  other arithmetic: 15.8 us -> 20.3 us
  starting transfers between devices: 23.2 us -> 27.7 us
    all_to_all x0 -> x1, blocking collectives: none -> 58.9 us  [on_device(): block_rows = lax.all_to_all(copies, 'tp', 0, 0, tiled=True)]
    all_gather x1 -> x0, waiting for transfers between devices: 58 us -> none  [on_device(): block_rows = lax.all_gather(stacked, 'tp', axis=0, tiled=True)]
    all_to_all x2, waiting for transfers between devices: 78.6 us -> 72.2 us  [summed_on_arrival(): lax.all_to_all(tiles, axis, split_axis=0, concat_axis=0, tiled=True)]
    all_to_all x1, starting transfers between devices: 12.4 us -> 17.2 us  [exchange_in_order(): lax.all_to_all(tiles, axes[k], split_axis=k, concat_axis=k, tiled=True)]
    concatenate x0 -> x1, other arithmetic: none -> 4.44 us  [on_device(): copies = jnp.concatenate([stacked] * lax.axis_size('tp'), axis=0)]
  transfers between devices with their start and end apart: 5 -> 4, of which waited for: 5 -> 4; matrix products, arithmetic and copies ran while one was open for 2% -> 2% of each run, Pallas kernels for 0% -> 0%
where the time goes in v1:
time: 398 us; the launch traced here: 397 us
  blocking collectives  157 us (39%)
  waiting for transfers between devices  134 us (34%)
  local copies, waits for them, and re-layouts  40.8 us (10%)
  starting transfers between devices  27.7 us (7%)
  other arithmetic  20.3 us (5%)
  matrix products  17.3 us (4%)
    all_to_all x3, blocking collectives, exchange_in_order(): lax.all_to_all(tiles, axes[k], split_axis=k, concat_axis=k, tiled=True)  98 us
    all_to_all x2, waiting for transfers between devices, summed_on_arrival(): lax.all_to_all(tiles, axis, split_axis=0, concat_axis=0, tiled=True)  72.2 us
    all_to_all x1, waiting for transfers between devices, exchange_in_order(): lax.all_to_all(tiles, axes[k], split_axis=k, concat_axis=k, tiled=True)  60.9 us
    all_to_all x1, blocking collectives, on_device(): block_rows = lax.all_to_all(copies, 'tp', 0, 0, tiled=True)  58.9 us
    all_to_all x1, starting transfers between devices, exchange_in_order(): lax.all_to_all(tiles, axes[k], split_axis=k, concat_axis=k, tiled=True)  17.2 us
    all_to_all x4, local copies, waits for them, and re-layouts, exchange_in_order(): lax.all_to_all(tiles, axes[k], split_axis=k, concat_axis=k, tiled=True)  9.04 us
    all_to_all x2, starting transfers between devices, summed_on_arrival(): lax.all_to_all(tiles, axis, split_axis=0, concat_axis=0, tiled=True)  8.97 us
    another operation x4, local copies, waits for them, and re-layouts, exchange_in_order(): tiles = tiles.reshape(*lengths, *tiles.shape[1:])  8.68 us
  transfers between devices with their start and end apart: 4, of which 4 were waited for; matrix products, arithmetic and copies ran while one was open for 2% of the time, Pallas kernels for 0%

profile of v1, /device:TPU:40, one launch (start us, length us, event | category | flops | bytes accessed | tf_op | source)
XLA Modules:
  0.0 397.4 jit_solution(10434689120648407630)
XLA Ops:
  0.6 0.0 copy-start
  0.6 0.9 copy.21
  1.6 0.1 eq.29
  1.7 0.1 eq.25
  1.9 0.7 broadcast_multiply_fusion
  2.6 0.6 reduce-window.6
  3.1 0.2 slice_reduce_fusion
  3.4 0.1 copy.20
  3.5 0.1 mul.102
  3.6 1.2 fusion.5
  4.9 1.2 fusion.7
  6.1 1.7 broadcast_in_dim.5
  7.8 2.3 reshape.95
  10.0 0.1 fusion.22
  10.1 4.0 scatter_custom_fusion
  14.1 3.3 reshape_reshape_reshape.12
  17.4 2.3 copy.24
  19.8 4.8 %all_to_all.42 = bf16[16,2,1,10,2048]{4,0,3,2,1:T(8,128)(2,1)S(1)} all-to-all(bf16[16,2,1,10,2048]{4,0,3,2,1:T(8,128)(2,1)S(1)} %copy.24), channel_id=1, replica_groups=mesh['grp'=2,'ep_0'=16,'ep_1'=2,'tp'=4] {'ep_1'}, dimensions={1} | all-to-all | bytes 2621440 | tf_op jit(solution)/shard_map/all_to_all | solution.py:42
  24.6 1.3 copy.25
  25.9 87.6 %all_to_all.43 = bf16[16,2,1,10,2048]{4,1,3,2,0:T(2,128)(2,1)S(1)} all-to-all(bf16[16,2,1,10,2048]{4,1,3,2,0:T(2,128)(2,1)S(1)} %copy.25), channel_id=1, replica_groups=mesh['grp'=2,'ep_0'=16,'ep_1'=2,'tp'=4] {'ep_0'}, dimensions={0} | all-to-all | bytes 2621440 | tf_op jit(solution)/shard_map/all_to_all | solution.py:42
  113.5 2.0 copy.26
  115.5 3.6 reshape_reshape_reshape.13
  119.1 4.4 %pad_maximum_fusion = bf16[1280,2048]{1,0:T(8,128)(2,1)S(1)} fusion(bf16[320,2048]{1,0:T(8,128)(2,1)} %reshape_reshape_reshape.13), kind=kLoop, calls=%fused_computation.3 | loop fusion | flops 20971520 | bytes 6553600 | tf_op jit(solution)/shard_map/concatenate | solution.py:108
  123.6 0.0 copy-start.8
  123.6 58.9 %all_to_all.44 = bf16[4,320,2048]{2,1,0:T(8,128)(2,1)S(1)} all-to-all(bf16[4,320,2048]{2,1,0:T(8,128)(2,1)S(1)} %bitcast.41), channel_id=1, replica_groups=mesh['grp'=2,'ep_0'=16,'ep_1'=2,'tp'=4] {'tp'}, dimensions={0} | all-to-all | bytes 10485760 | tf_op jit(solution)/shard_map/all_to_all | solution.py:109
  182.5 0.0 copy-done.8
  182.5 0.0 copy-start.9
  182.5 4.3 %fusion.3 = f32[1280,768]{1,0:T(8,128)S(1)} fusion(bf16[1280,2048]{1,0:T(8,128)(2,1)S(1)} %bitcast.43, bf16[1,2048,768]{2,1,0:T(8,128)(2,1)S(1)} %copy-done.8), kind=kOutput, calls=%fused_computation.8 | convolution fusion | flops 4026531840 | bytes 12320768 | tf_op jit(solution)/shard_map/dot_general | solution.py:110
  186.8 0.0 copy-done.9
  186.8 4.8 %fusion = bf16[1280,768]{1,0:T(8,128)(2,1)S(1)} fusion(bf16[1280,2048]{1,0:T(8,128)(2,1)S(1)} %bitcast.44, f32[1280,768]{1,0:T(8,128)S(1)} %fusion.3, bf16[1,2048,768]{2,1,0:T(8,128)(2,1)S(1)} %copy-done.9), kind=kOutput, calls=%fused_computation.5 | convolution fusion | flops 4032430080 | bytes 14286848 | tf_op jit(solution)/shard_map/dot_general | solution.py:111
  191.6 0.0 copy-done
  191.7 6.1 %convolution_convert_fusion = bf16[1280,2048]{1,0:T(8,128)(2,1)} fusion(bf16[1280,768]{1,0:T(8,128)(2,1)S(1)} %fusion, bf16[1,768,2048]{2,1,0:T(8,128)(2,1)S(1)} %copy-done), kind=kOutput, calls=%fused_computation.2 | convolution fusion | flops 4029153280 | bytes 10354688 | tf_op jit(solution)/shard_map/dot_general | solution.py:114
  197.7 0.0 copy-start.4
  197.7 0.0 copy-start.3
  197.7 5.3 %all-to-all-start.4 = ((bf16[4,320,2048]{2,1,0:T(8,128)(2,1)}), bf16[4,320,2048]{2,1,0:T(8,128)(2,1)}, u32[]{:S(2)}, u32[]{:S(2)}) async-start(bf16[4,320,2048]{2,1,0:T(8,128)(2,1)} %bitcast.42), calls=%async_computation.4 | async-start | bytes 10485760 | tf_op jit(solution)/shard_map/all_to_all | solution.py:28
  203.0 0.0 copy-done.4
  203.0 0.0 copy-done.5
  203.0 0.1 convert_multiply_fusion.2
  203.1 1.5 collective-permute-start
  204.6 0.0 copy-done.6
  204.7 0.6 collective-permute-done
  205.2 0.0 copy-done.2
  205.2 0.0 copy-done.3
  205.2 2.1 convolution_convert_fusion.1
  207.3 49.1 %all-to-all-done.4 = bf16[4,320,2048]{2,1,0:T(8,128)(2,1)} async-done(((bf16[4,320,2048]{2,1,0:T(8,128)(2,1)}), bf16[4,320,2048]{2,1,0:T(8,128)(2,1)}, u32[]{:S(2)}, u32[]{:S(2)}) %all-to-all-start.4) | async-done | bytes 5242912 | tf_op jit(solution)/shard_map/all_to_all | solution.py:28
  256.4 5.0 %reduce_sum.57 = bf16[320,2048]{1,0:T(8,128)(2,1)} reduce(bf16[4,320,2048]{2,1,0:T(8,128)(2,1)} %all-to-all-done.4, bf16[]{:T(256)} %constant.9.clone.1), dimensions={0}, to_apply=%region_6.7 | reduce | flops 1966080 | bytes 6553602 | tf_op jit(solution)/shard_map/reduce_sum | solution.py:29
  261.4 2.3 reshape_reshape_reshape.14
  263.7 0.7 copy.27
  264.5 5.6 %all_to_all.45 = bf16[16,2,1,10,2048]{4,0,3,2,1:T(8,128)(2,1)} all-to-all(bf16[16,2,1,10,2048]{4,0,3,2,1:T(8,128)(2,1)S(1)} %copy.27), channel_id=1, replica_groups=mesh['grp'=2,'ep_0'=16,'ep_1'=2,'tp'=4] {'ep_1'}, dimensions={1} | all-to-all | bytes 2621440 | tf_op jit(solution)/shard_map/all_to_all | solution.py:42
  270.1 3.7 all-to-all-start
  273.8 0.0 copy-start.7
  273.8 3.7 copy.28
  277.6 23.1 %all-to-all-done = bf16[4,128,2048]{2,1,0:T(8,128)(2,1)S(1)} async-done(((bf16[4,128,2048]{2,1,0:T(8,128)(2,1)}), bf16[4,128,2048]{2,1,0:T(8,128)(2,1)S(1)}, u32[]{:S(2)}, u32[]{:S(2)}) %all-to-all-start) | async-done | bytes 2097184 | tf_op jit(solution)/shard_map/all_to_all | solution.py:28
  300.6 17.2 %all-to-all-start.6 = ((bf16[16,2,1,10,2048]{4,1,3,2,0:T(2,128)(2,1)}), bf16[16,2,1,10,2048]{4,1,3,2,0:T(2,128)(2,1)}, u32[]{:S(2)}, u32[]{:S(2)}) async-start(bf16[16,2,1,10,2048]{4,1,3,2,0:T(2,128)(2,1)} %copy.28), calls=%async_computation.6 | async-start | bytes 2621440 | tf_op jit(solution)/shard_map/all_to_all | solution.py:42
  317.8 0.0 copy-done.7
  317.8 0.1 copy.30
  317.9 1.3 reduce_sum.53
  319.3 60.9 %all-to-all-done.6 = bf16[16,2,1,10,2048]{4,1,3,2,0:T(2,128)(2,1)} async-done(((bf16[16,2,1,10,2048]{4,1,3,2,0:T(2,128)(2,1)}), bf16[16,2,1,10,2048]{4,1,3,2,0:T(2,128)(2,1)}, u32[]{:S(2)}, u32[]{:S(2)}) %all-to-all-start.6) | async-done | bytes 1310752 | tf_op jit(solution)/shard_map/all_to_all | solution.py:42
  380.2 2.0 copy.29
  382.1 1.3 reshape_reshape_reshape.15
  383.5 5.0 %gather_fusion = bf16[256,2048]{1,0:T(8,128)(2,1)} fusion(bf16[320,2048]{1,0:T(8,128)(2,1)} %reshape_reshape_reshape.15, s32[1024]{0:T(1024)S(1)} %pad_clamp_fusion), kind=kCustom, calls=%fused_computation | custom fusion | bytes 2098176 | tf_op jit(solution)/shard_map/gather | solution.py:121
  388.5 3.4 reshape.82
  391.9 5.6 %multiply_reduce_fusion = bf16[128,2048]{1,0:T(8,128)(2,1)} fusion(f32[128,2,2048]{2,1,0:T(2,128)} %reshape.82, f32[128,2]{1,0:T(8,128)S(1)} %copy.30), kind=kLoop, calls=%fused_computation.11 | loop fusion | flops 786432 | bytes 2622464 | tf_op jit(solution)/shard_map/reduce_sum | solution.py:123
  397.4 0.0 copy-done.1
  (12 shorter events, 0.1 us)
Async XLA Ops:
  0.6 191.0 %copy-start = (bf16[1,768,2048]{2,1,0:T(8,128)(2,1)S(1)}, bf16[1,768,2048]{2,1,0:T(8,128)(2,1)}, u32[]{:S(2)}) copy-start(bf16[1,768,2048]{2,1,0:T(8,128)(2,1)} %param.23) | copy-start | bytes 9437188
  123.6 58.9 %copy-start.8 = (bf16[1,2048,768]{2,1,0:T(8,128)(2,1)S(1)}, bf16[1,2048,768]{2,1,0:T(8,128)(2,1)}, u32[]{:S(2)}) copy-start(bf16[1,2048,768]{2,1,0:T(8,128)(2,1)} %param.21) | copy-start | bytes 9437188
  182.5 4.3 %copy-start.9 = (bf16[1,2048,768]{2,1,0:T(8,128)(2,1)S(1)}, bf16[1,2048,768]{2,1,0:T(8,128)(2,1)}, u32[]{:S(2)}) copy-start(bf16[1,2048,768]{2,1,0:T(8,128)(2,1)} %param.22) | copy-start | bytes 9437188
  197.7 5.3 %copy-start.4 = (bf16[512,256]{1,0:T(8,128)(2,1)S(1)}, bf16[512,256]{1,0:T(8,128)(2,1)}, u32[]{:S(2)}) copy-start(bf16[512,256]{1,0:T(8,128)(2,1)} %param.14) | copy-start | bytes 786436
  197.7 5.3 %copy-start.5 = (bf16[512,256]{1,0:T(8,128)(2,1)S(1)}, bf16[512,256]{1,0:T(8,128)(2,1)}, u32[]{:S(2)}) copy-start(bf16[512,256]{1,0:T(8,128)(2,1)} %param.13) | copy-start | bytes 786436
  197.7 6.9 %copy-start.6 = (f32[3,256]{1,0:T(4,128)S(1)}, f32[3,256]{1,0:T(4,128)}, u32[]{:S(2)}) copy-start(f32[3,256]{1,0:T(4,128)} %param.15) | copy-start | bytes 9220
  197.7 7.5 %copy-start.2 = (bf16[256,2048]{1,0:T(8,128)(2,1)S(1)}, bf16[256,2048]{1,0:T(8,128)(2,1)}, u32[]{:S(2)}) copy-start(bf16[256,2048]{1,0:T(8,128)(2,1)} %param.16) | copy-start | bytes 3145732
  197.7 7.5 %copy-start.3 = (bf16[512,256]{1,0:T(8,128)(2,1)S(1)}, bf16[512,256]{1,0:T(8,128)(2,1)}, u32[]{:S(2)}) copy-start(bf16[512,256]{1,0:T(8,128)(2,1)} %param.12) | copy-start | bytes 786436
  197.7 58.7 %all-to-all-start.4 = ((bf16[4,320,2048]{2,1,0:T(8,128)(2,1)}), bf16[4,320,2048]{2,1,0:T(8,128)(2,1)}, u32[]{:S(2)}, u32[]{:S(2)}) async-start(bf16[4,320,2048]{2,1,0:T(8,128)(2,1)} %bitcast.42), calls=%async_computation.4 | async-start | bytes 10485760 | tf_op jit(solution)/shard_map/all_to_all | solution.py:28
  203.1 2.1 collective-permute-start
  270.1 30.5 %all-to-all-start = ((bf16[4,128,2048]{2,1,0:T(8,128)(2,1)}), bf16[4,128,2048]{2,1,0:T(8,128)(2,1)S(1)}, u32[]{:S(2)}, u32[]{:S(2)}) async-start(bf16[4,128,2048]{2,1,0:T(8,128)(2,1)} %bitcast.3), calls=%async_computation | async-start | bytes 4194304 | tf_op jit(solution)/shard_map/all_to_all | solution.py:28
  273.8 44.0 %copy-start.7 = (f32[128,2]{0,1:T(2,128)S(1)}, f32[128,2]{0,1:T(2,128)}, u32[]{:S(2)}) copy-start(f32[128,2]{0,1:T(2,128)} %param.20) | copy-start | bytes 3076
  300.6 79.5 %all-to-all-start.6 = ((bf16[16,2,1,10,2048]{4,1,3,2,0:T(2,128)(2,1)}), bf16[16,2,1,10,2048]{4,1,3,2,0:T(2,128)(2,1)}, u32[]{:S(2)}, u32[]{:S(2)}) async-start(bf16[16,2,1,10,2048]{4,1,3,2,0:T(2,128)(2,1)} %copy.28), calls=%async_computation.6 | async-start | bytes 2621440 | tf_op jit(solution)/shard_map/all_to_all | solution.py:42
  383.5 14.0 %copy-start.1 = (bf16[1,768,2048]{2,1,0:T(8,128)(2,1)S(1)}, bf16[1,768,2048]{2,1,0:T(8,128)(2,1)}, u32[]{:S(2)}) copy-start(bf16[1,768,2048]{2,1,0:T(8,128)(2,1)} %param.23) | copy-start | bytes 9437188
